TPU v7x, 512 devices: a 8x2x16 block of a 8x8x16 slice. The times are simulated.
512 devices in a mesh: grp: 2 (over y), ep: 32 (over z, core), tp: 8 (over x).
Axes of the slice: x: 8, y: 2, z: 16, core: 2. Of those that a mesh axis runs over, the one named last changes fastest.
The devices are a block of a 8x8x16 slice.
Arguments:
- tokens: bfloat16 [16384, 2048], P(('grp', 'ep'), 'tp'), parts along dimension 0, may hold values from -6 to 6
- norm_gain: float32 [2048], replicated, may hold values from 0.1 to 1.9
- expert_ids: int32 [16384, 2], P(('grp', 'ep')), parts along dimension 0, may hold values from 0 to 31, all different within a row; in each aligned block of 256 rows (0 to 255, 256 to 511, ...) at most 24 rows name the same one
- gate_weights: float32 [16384, 2], P(('grp', 'ep')), parts along dimension 0, may hold values from 0.25 to 1
- w_gate: bfloat16 [32, 2048, 3072], P('ep', None, 'tp'), may hold values from -0.125 to 0.125
- w_up: bfloat16 [32, 2048, 3072], P('ep', None, 'tp'), may hold values from -0.125 to 0.125
- w_down: bfloat16 [32, 3072, 2048], P('ep', 'tp'), may hold values from -0.15625 to 0.15625
Outputs:
- mixed: bfloat16 [16384, 2048], P(('grp', 'ep'), 'tp'), parts along dimension 0
There are 2 independent parts, one for each index of `grp`. A program takes and returns all parts, laid end to end along the dimension named above; an argument that names none is the same for every part. Nothing has to cross between parts.
Inputs may be any that keep to these rules, and one draw needn't show every extreme that they name: `expert_ids`: each token names 2 different experts. Within the 256 rows of one index of ep (aligned blocks) no expert is named more than 24 times, and in some blocks one expert is named exactly 24 times.
All inputs are finite; a program needn't handle non-finite values.
Results may differ from a plain program's by a relative error of at most 0.015.
Values may be sent and summed in bfloat16 or wider, within the bound.
A program may use at most 64 MiB of HBM per device.

v0:
```python
import jax
import jax.numpy as jnp
from jax import lax
from jax.sharding import Mesh
from jax.sharding import PartitionSpec as P

EP = ("ep_0", "ep_1")
GRP_EP = ("grp", "ep_0", "ep_1")
epsilon = 1e-06


def sent_to_all(array, axis):
    count = lax.axis_size(axis)
    return lax.all_to_all(
        jnp.broadcast_to(array[None], (count, *array.shape)), axis, 0, 0, tiled=True
    )


def over_copies(array, axis):
    everything = sent_to_all(array, axis)
    return jnp.sum(everything, axis=0)


def in_blocks(array, dim, count):
    dims = array.shape
    blocks = array.reshape(*dims[:dim], count, dims[dim] // count, *dims[dim + 1 :])
    return jnp.moveaxis(blocks, dim, 0)


def joined_along(blocks, dim):
    dims = list(blocks.shape[1:])
    dims[dim] *= blocks.shape[0]
    return jnp.moveaxis(blocks, 0, dim).reshape(dims)


def moved_by_axis(blocks, axes, order):
    inside = blocks.shape[1:]
    whole = blocks.reshape(*(lax.axis_size(a) for a in axes), *inside)
    for k in order:
        whole = lax.all_to_all(whole, axes[k], k, k, tiled=True)
    return whole.reshape(-1, *inside)


def core_and_chips(array, groups, order, split_dim, concat_dim):
    count = lax.axis_size(groups[0]) * lax.axis_size(groups[1])
    blocks = in_blocks(array, split_dim, count)
    return joined_along(moved_by_axis(blocks, groups, order), concat_dim)


def on_device(tokens, norm_gain, expert_ids, gate_weights, w_gate, w_up, w_down):
    tok_count = tokens.shape[0]
    top_count = expert_ids.shape[1]
    expert_count = lax.axis_size(EP)
    capacity = 3 * tok_count * top_count // (2 * expert_count)
    model_width = norm_gain.shape[0]
    flat_ids = expert_ids.reshape(-1)
    onehot = (flat_ids[:, None] == jnp.arange(expert_count, dtype=jnp.int32)[None, :]).astype(
        jnp.int32
    )
    earlier = jnp.cumsum(onehot, axis=0) - onehot
    slot_index = jnp.sum(earlier * onehot, axis=1)
    dest_index = flat_ids * capacity + slot_index
    owner_index = jnp.arange(tok_count * top_count, dtype=jnp.int32) // top_count
    slot_token = (
        jnp.full((expert_count * capacity,), tok_count, jnp.int32).at[dest_index].set(owner_index)
    )
    tok_values = tokens.astype(jnp.float32)
    square_sum = over_copies(jnp.sum(tok_values * tok_values, axis=1, keepdims=True), "tp")
    col_count = tokens.shape[1]
    gain_part = lax.dynamic_slice_in_dim(norm_gain, lax.axis_index("tp") * col_count, col_count)
    normed = (tok_values * lax.rsqrt(square_sum / model_width + epsilon) * gain_part).astype(
        jnp.bfloat16
    )
    buffer = jnp.take(normed, slot_token, axis=0, mode="fill", fill_value=0).reshape(
        expert_count, capacity, -1
    )
    received = core_and_chips(buffer, ("ep_0", "ep_1"), (1, 0), 0, 0)
    source_count, item_count, col_count = received.shape
    tok_rows = received.reshape(-1, col_count)
    col_piece = lax.all_gather(tok_rows, "tp", axis=1, tiled=True)
    gate_rows = w_gate[0]
    up_rows = w_up[0]
    gate_part = jnp.dot(col_piece, gate_rows, preferred_element_type=jnp.float32)
    up_part = jnp.dot(col_piece, up_rows, preferred_element_type=jnp.float32)
    hidden = (jax.nn.silu(gate_part) * up_part).astype(jnp.bfloat16)
    partial_value = jnp.dot(hidden, w_down[0], preferred_element_type=jnp.float32)
    partial_value = partial_value.reshape(source_count, item_count, -1)
    summed = lax.psum_scatter(
        partial_value.astype(jnp.bfloat16), "tp", scatter_dimension=2, tiled=True
    )
    came_back = lax.all_to_all(summed, EP, split_axis=0, concat_axis=0, tiled=True)
    picked = came_back.reshape(expert_count * capacity, -1)[dest_index].astype(jnp.float32)
    weighted = picked * gate_weights.reshape(-1)[:, None]
    return jnp.sum(weighted.reshape(tok_count, top_count, -1), axis=1).astype(jnp.bfloat16)


def solution(mesh):
    finer = Mesh(
        mesh.devices.reshape(mesh.shape["grp"], 16, 2, mesh.shape["tp"]),
        ("grp", "ep_0", "ep_1", "tp"),
    )
    in_specs = (
        P(GRP_EP, "tp"),
        P(),
        P(GRP_EP, None),
        P(GRP_EP, None),
        P(EP, None, "tp"),
        P(EP, None, "tp"),
        P(EP, "tp", None),
    )
    out_specs = P(GRP_EP, "tp")
    return jax.shard_map(
        on_device, mesh=finer, in_specs=in_specs, out_specs=out_specs, check_vma=False
    )
```

profile of v0, /device:TPU:65, one launch (start us, length us, event | category | flops | bytes accessed | tf_op | source)
XLA Modules:
  0.0 271.2 jit_solution(14151282188558710371)
XLA Ops:
  6.5 0.0 copy-start
  6.6 1.1 fusion.11
  7.7 0.6 broadcast_in_dim.29
  8.3 7.9 %all-to-all-start = ((f32[8,256,1]{1,2,0:T(1,128)}), f32[8,256,1]{1,2,0:T(1,128)S(1)}, u32[]{:S(2)}, u32[]{:S(2)}) async-start(f32[8,256,1]{1,2,0:T(1,128)} %broadcast_in_dim.29), calls=%async_computation | async-start | bytes 16384 | tf_op jit(solution)/shard_map/all_to_all | solution.py:14
  16.2 0.1 all-gather.2.cloned.1.call-start
  16.2 0.8 copy.15
  17.0 0.1 eq.29
  17.2 0.1 eq.25
  17.3 0.7 broadcast_multiply_fusion
  18.0 1.2 reduce-window.6
  19.2 0.2 slice_reduce_fusion
  19.5 0.1 copy.14
  19.6 0.1 mul.59
  19.8 0.1 fusion.16
  19.9 2.4 scatter_custom_fusion
  22.4 0.1 broadcast_in_dim.27
  22.5 0.8 dynamic_slice.3
  23.3 0.0 all-to-all-done
  23.3 1.0 fusion.13
  24.3 2.7 gather_fusion
  27.0 0.2 copy_select_fusion
  27.1 0.0 copy-start.3
  27.2 41.3 %all_to_all.20 = bf16[16,2,1,24,256]{4,3,0,2,1:T(8,128)(2,1)S(1)} all-to-all(bf16[16,2,1,24,256]{4,3,0,2,1:T(8,128)(2,1)S(1)} %copy_select_fusion), channel_id=1, replica_groups=mesh['grp'=2,'ep_0'=16,'ep_1'=2,'tp'=8] {'ep_1'}, dimensions={1} | all-to-all | bytes 786432 | tf_op jit(solution)/shard_map/all_to_all | solution.py:40
  68.5 24.6 %all_to_all.21 = bf16[16,2,1,24,256]{4,3,1,2,0:T(8,128)(2,1)} all-to-all(bf16[16,2,1,24,256]{4,3,1,2,0:T(8,128)(2,1)S(1)} %copy.20), channel_id=1, replica_groups=mesh['grp'=2,'ep_0'=16,'ep_1'=2,'tp'=8] {'ep_0'}, dimensions={0} | all-to-all | bytes 786432 | tf_op jit(solution)/shard_map/all_to_all | solution.py:40
  93.1 0.1 all-gather.2.cloned.1.call-update
  93.2 0.1 reduce-scatter.2.cloned.1.call-start
  93.3 59.5 %all-gather.2.cloned.1.call-done = bf16[768,2048]{1,0:T(8,128)(2,1)} async-done(((bf16[768,256]{1,0:T(8,128)(2,1)}), bf16[768,2048]{1,0:T(8,128)(2,1)}) %all-gather.2.cloned.1.call-update) | async-done | bytes 3145744 | tf_op jit(solution)/shard_map/all_gather | solution.py:80
  152.8 0.0 copy-done.3
  152.8 0.0 copy-start.2
  152.8 0.0 copy-start.4
  152.8 3.8 %fusion.3 = f32[768,384]{1,0:T(8,128)S(1)} fusion(bf16[768,2048]{1,0:T(8,128)(2,1)} %all-gather.2.cloned.1.call-done, bf16[1,2048,384]{2,1,0:T(8,128)(2,1)S(1)} %copy-done.3), kind=kOutput, calls=%fused_computation.7 | convolution fusion | flops 1207959552 | bytes 5898240 | tf_op jit(solution)/shard_map/dot_general | solution.py:83
  156.6 0.0 copy-done.2
  156.6 0.0 copy-done.4
  156.6 1.8 fusion.8
  158.5 0.0 copy-done
  158.5 3.5 %convolution_convert_fusion = bf16[32,24,2048]{2,1,0:T(8,128)(2,1)} fusion(bf16[32,24,384]{2,1,0:T(8,128)(2,1)S(1)} %bitcast.48, bf16[1,384,2048]{2,1,0:T(8,128)(2,1)S(1)} %copy-done), kind=kOutput, calls=%fused_computation.3 | convolution fusion | flops 1209532416 | bytes 5308416 | tf_op jit(solution)/shard_map/dot_general | solution.py:86
  162.0 0.0 copy-start.1
  162.0 0.1 reduce-scatter.2.cloned.1.call-update
  162.0 54.2 %reduce-scatter.2.cloned.1.call-done = bf16[32,24,256]{2,1,0:T(8,128)(2,1)} async-done(((bf16[32,24,2048]{2,1,0:T(8,128)(2,1)}), bf16[32,24,256]{2,1,0:T(8,128)(2,1)}) %reduce-scatter.2.cloned.1.call-update) | async-done | bytes 393232 | tf_op jit(solution)/shard_map/reduce_scatter | solution.py:88
  216.2 16.9 %all-to-all-start.3 = ((bf16[32,24,256]{2,1,0:T(8,128)(2,1)}), bf16[32,24,256]{2,1,0:T(8,128)(2,1)S(1)}, u32[]{:S(2)}, u32[]{:S(2)}) async-start(bf16[32,24,256]{2,1,0:T(8,128)(2,1)} %reduce-scatter.2.cloned.1.call-done), calls=%async_computation.4 | async-start | bytes 786432 | tf_op jit(solution)/shard_map/all_to_all | solution.py:91
  233.2 0.0 copy-done.1
  233.2 0.1 copy.21
  233.3 27.4 %all-to-all-done.3 = bf16[32,24,256]{2,1,0:T(8,128)(2,1)S(1)} async-done(((bf16[32,24,256]{2,1,0:T(8,128)(2,1)}), bf16[32,24,256]{2,1,0:T(8,128)(2,1)S(1)}, u32[]{:S(2)}, u32[]{:S(2)}) %all-to-all-start.3) | async-done | bytes 393248 | tf_op jit(solution)/shard_map/all_to_all | solution.py:91
  260.7 1.9 gather_fusion.1
  262.7 0.3 reshape.98
  262.9 1.4 multiply_reduce_fusion
  (13 shorter events, 0.2 us)
Async XLA Ops:
  6.5 152.0 %copy-start = (bf16[1,384,2048]{2,1,0:T(8,128)(2,1)S(1)}, bf16[1,384,2048]{2,1,0:T(8,128)(2,1)}, u32[]{:S(2)}) copy-start(bf16[1,384,2048]{2,1,0:T(8,128)(2,1)} %param.13) | copy-start | bytes 4718596
  8.3 15.0 %all-to-all-start = ((f32[8,256,1]{1,2,0:T(1,128)}), f32[8,256,1]{1,2,0:T(1,128)S(1)}, u32[]{:S(2)}, u32[]{:S(2)}) async-start(f32[8,256,1]{1,2,0:T(1,128)} %broadcast_in_dim.29), calls=%async_computation | async-start | bytes 16384 | tf_op jit(solution)/shard_map/all_to_all | solution.py:14
  16.2 136.6 %all-gather.2.cloned.1.call-start = ((), (), s32[]{:S(2)}) async-start(), calls=%async_computation.5 | async-start | bytes 3538944 | tf_op jit(solution)/shard_map/all_gather | solution.py:80
  27.1 125.6 %copy-start.3 = (bf16[1,2048,384]{2,1,0:T(8,128)(2,1)S(1)}, bf16[1,2048,384]{2,1,0:T(8,128)(2,1)}, u32[]{:S(2)}) copy-start(bf16[1,2048,384]{2,1,0:T(8,128)(2,1)} %param.11) | copy-start | bytes 4718596
  93.2 123.0 %reduce-scatter.2.cloned.1.call-start = ((), (), s32[]{:S(2)}) async-start(), calls=%async_computation.6 | async-start | bytes 3538944 | tf_op jit(solution)/shard_map/reduce_scatter | solution.py:88
  152.8 3.8 %copy-start.2 = (bf16[768,2048]{1,0:T(8,128)(2,1)S(1)}, bf16[768,2048]{1,0:T(8,128)(2,1)}, u32[]{:S(2)}) copy-start(bf16[768,2048]{1,0:T(8,128)(2,1)} %all-gather.2.cloned.1.call-done) | copy-start | bytes 9437188
  152.8 3.8 %copy-start.4 = (bf16[1,2048,384]{2,1,0:T(8,128)(2,1)S(1)}, bf16[1,2048,384]{2,1,0:T(8,128)(2,1)}, u32[]{:S(2)}) copy-start(bf16[1,2048,384]{2,1,0:T(8,128)(2,1)} %param.12) | copy-start | bytes 4718596
  162.0 71.2 %copy-start.1 = (f32[256,2]{0,1:T(2,128)S(1)}, f32[256,2]{0,1:T(2,128)}, u32[]{:S(2)}) copy-start(f32[256,2]{0,1:T(2,128)} %param.10) | copy-start | bytes 6148
  216.2 44.5 %all-to-all-start.3 = ((bf16[32,24,256]{2,1,0:T(8,128)(2,1)}), bf16[32,24,256]{2,1,0:T(8,128)(2,1)S(1)}, u32[]{:S(2)}, u32[]{:S(2)}) async-start(bf16[32,24,256]{2,1,0:T(8,128)(2,1)} %reduce-scatter.2.cloned.1.call-done), calls=%async_computation.4 | async-start | bytes 786432 | tf_op jit(solution)/shard_map/all_to_all | solution.py:91
Sparse Core Ops, SparseCore 0:
  93.3 59.4 all-gather.1
  162.2 54.0 reduce-scatter.1
where the time goes:
time: 272 us; the launch traced here: 271 us
  waiting for transfers between devices  141 us (52%)
  blocking collectives  65.9 us (24%)
  starting transfers between devices  24.9 us (9%)
  between operations  13.6 us (5%)
  local copies, waits for them, and re-layouts  10.6 us (4%)
  matrix products  9.14 us (3%)
  other arithmetic  5.77 us (2%)
    all_to_all x2, blocking collectives, moved_by_axis(): whole = lax.all_to_all(whole, axes[k], k, k, tiled=True)  65.9 us
    all_gather x1, waiting for transfers between devices, on_device(): col_piece = lax.all_gather(tok_rows, 'tp', axis=1, tiled=True)  59.5 us
    reduce_scatter x1, waiting for transfers between devices, on_device(): lax.psum_scatter(partial_value.astype(jnp.bfloat16), 'tp', scatter_dimens...  54.2 us
    all_to_all x1, waiting for transfers between devices, on_device(): lax.all_to_all(summed, EP, split_axis=0, concat_axis=0, tiled=True)  27.4 us
    all_to_all x1, starting transfers between devices, on_device(): lax.all_to_all(summed, EP, split_axis=0, concat_axis=0, tiled=True)  16.9 us
    all_to_all x1, starting transfers between devices, sent_to_all(): lax.all_to_all(jnp.broadcast_to(array[None], (count, *array.shape)), axis...  7.86 us
  transfers between devices with their start and end apart: 4, of which 3 were waited for; matrix products, arithmetic and copies ran while one was open for 3% of the time, Pallas kernels for 0%

commit v1 on v0

--- a/solution.py
+++ b/solution.py
@@ -77,7 +77,10 @@
     received = core_and_chips(buffer, ("ep_0", "ep_1"), (1, 0), 0, 0)
     source_count, item_count, col_count = received.shape
     tok_rows = received.reshape(-1, col_count)
-    col_piece = lax.all_gather(tok_rows, "tp", axis=1, tiled=True)
+    count_2 = lax.axis_size("tp")
+    tiles = jnp.stack([tok_rows for _ in range(count_2)])
+    tiles = lax.all_to_all(tiles, "tp", split_axis=0, concat_axis=0)
+    col_piece = jnp.concatenate(tiles, axis=1)
     gate_rows = w_gate[0]
     up_rows = w_up[0]
     gate_part = jnp.dot(col_piece, gate_rows, preferred_element_type=jnp.float32)

time: 272 us -> 284 us (1.044)
  blocking collectives: 65.9 us -> 137 us
  waiting for transfers between devices: 141 us -> 84.1 us
    all_to_all x0 -> x1, blocking collectives: none -> 71.4 us  [on_device(): tiles = lax.all_to_all(tiles, 'tp', split_axis=0, concat_axis=0)]
    all_gather x1 -> x0, waiting for transfers between devices: 59.5 us -> none  [on_device(): col_piece = lax.all_gather(tok_rows, 'tp', axis=1, tiled=True)]
  transfers between devices with their start and end apart: 4 -> 3, of which waited for: 3 -> 2; matrix products, arithmetic and copies ran while one was open for 3% -> 3% of each run, Pallas kernels for 0% -> 0%
where the time goes in v1:
time: 284 us; the launch traced here: 283 us
  blocking collectives  137 us (48%)
  waiting for transfers between devices  84.1 us (30%)
  starting transfers between devices  24.7 us (9%)
  between operations  13.6 us (5%)
  local copies, waits for them, and re-layouts  10.9 us (4%)
  matrix products  7.16 us (3%)
  other arithmetic  5.77 us (2%)
    all_to_all x1, blocking collectives, on_device(): tiles = lax.all_to_all(tiles, 'tp', split_axis=0, concat_axis=0)  71.4 us
    all_to_all x2, blocking collectives, moved_by_axis(): whole = lax.all_to_all(whole, axes[k], k, k, tiled=True)  65.7 us
    reduce_scatter x1, waiting for transfers between devices, on_device(): lax.psum_scatter(partial_value.astype(jnp.bfloat16), 'tp', scatter_dimens...  56.7 us
    all_to_all x1, waiting for transfers between devices, on_device(): lax.all_to_all(summed, EP, split_axis=0, concat_axis=0, tiled=True)  27.4 us
    all_to_all x1, starting transfers between devices, on_device(): lax.all_to_all(summed, EP, split_axis=0, concat_axis=0, tiled=True)  16.8 us
    all_to_all x1, starting transfers between devices, sent_to_all(): lax.all_to_all(jnp.broadcast_to(array[None], (count, *array.shape)), axis...  7.86 us
  transfers between devices with their start and end apart: 3, of which 2 were waited for; matrix products, arithmetic and copies ran while one was open for 3% of the time, Pallas kernels for 0%

profile of v1, /device:TPU:65, one launch (start us, length us, event | category | flops | bytes accessed | tf_op | source)
XLA Modules:
  0.0 283.4 jit_solution(5267630439003754427)
XLA Ops:
  6.5 0.0 copy-start
  6.6 1.1 fusion.11
  7.7 0.6 broadcast_in_dim.29
  8.3 7.9 %all-to-all-start = ((f32[8,256,1]{1,2,0:T(1,128)}), f32[8,256,1]{1,2,0:T(1,128)S(1)}, u32[]{:S(2)}, u32[]{:S(2)}) async-start(f32[8,256,1]{1,2,0:T(1,128)} %broadcast_in_dim.29), calls=%async_computation | async-start | bytes 16384 | tf_op jit(solution)/shard_map/all_to_all | solution.py:14
  16.2 0.1 reduce-scatter.2.cloned.1.call-start
  16.2 0.8 copy.16
  17.0 0.1 eq.29
  17.2 0.1 eq.25
  17.3 0.7 broadcast_multiply_fusion
  18.0 1.2 reduce-window.6
  19.2 0.2 slice_reduce_fusion
  19.5 0.1 copy.15
  19.6 0.1 mul.59
  19.8 0.1 fusion.16
  19.9 2.4 scatter_custom_fusion
  22.4 0.1 broadcast_in_dim.27
  22.5 0.8 dynamic_slice.3
  23.3 0.0 all-to-all-done
  23.3 1.0 fusion.13
  24.3 2.7 gather_fusion
  27.0 0.2 copy_select_fusion
  27.1 41.2 %all_to_all.25 = bf16[16,2,1,24,256]{4,3,0,2,1:T(8,128)(2,1)S(1)} all-to-all(bf16[16,2,1,24,256]{4,3,0,2,1:T(8,128)(2,1)S(1)} %copy_select_fusion), channel_id=1, replica_groups=mesh['grp'=2,'ep_0'=16,'ep_1'=2,'tp'=8] {'ep_1'}, dimensions={1} | all-to-all | bytes 786432 | tf_op jit(solution)/shard_map/all_to_all | solution.py:40
  68.4 24.5 %all_to_all.26 = bf16[16,2,1,24,256]{4,3,1,2,0:T(8,128)(2,1)S(1)} all-to-all(bf16[16,2,1,24,256]{4,3,1,2,0:T(8,128)(2,1)S(1)} %copy.21), channel_id=1, replica_groups=mesh['grp'=2,'ep_0'=16,'ep_1'=2,'tp'=8] {'ep_0'}, dimensions={0} | all-to-all | bytes 786432 | tf_op jit(solution)/shard_map/all_to_all | solution.py:40
  92.9 0.2 copy.22
  93.1 0.2 stack.3
  93.3 0.0 copy-start.1
  93.3 71.4 %all_to_all.27 = bf16[8,768,256]{1,2,0:T(8,128)(2,1)S(1)} all-to-all(bf16[8,768,256]{1,2,0:T(8,128)(2,1)S(1)} %stack.3), channel_id=1, replica_groups=mesh['grp'=2,'ep_0'=16,'ep_1'=2,'tp'=8] {'tp'}, dimensions={0} | all-to-all | bytes 6291456 | tf_op jit(solution)/shard_map/all_to_all | solution.py:82
  164.6 0.0 copy-done.1
  164.6 0.0 copy-start.3
  164.6 1.8 fusion.3
  166.5 0.0 copy-done.3
  166.5 1.9 fusion.8
  168.3 0.0 copy-done
  168.4 3.5 %convolution_convert_fusion = bf16[32,24,2048]{2,1,0:T(8,128)(2,1)} fusion(bf16[32,24,384]{2,1,0:T(8,128)(2,1)S(1)} %bitcast.53, bf16[1,384,2048]{2,1,0:T(8,128)(2,1)S(1)} %copy-done), kind=kOutput, calls=%fused_computation.3 | convolution fusion | flops 1209532416 | bytes 5308416 | tf_op jit(solution)/shard_map/dot_general | solution.py:89
  171.8 0.0 copy-start.2
  171.8 0.1 reduce-scatter.2.cloned.1.call-update
  171.9 56.7 %reduce-scatter.2.cloned.1.call-done = bf16[32,24,256]{2,1,0:T(8,128)(2,1)} async-done(((bf16[32,24,2048]{2,1,0:T(8,128)(2,1)}), bf16[32,24,256]{2,1,0:T(8,128)(2,1)}) %reduce-scatter.2.cloned.1.call-update) | async-done | bytes 393232 | tf_op jit(solution)/shard_map/reduce_scatter | solution.py:91
  228.6 16.8 %all-to-all-start.4 = ((bf16[32,24,256]{2,1,0:T(8,128)(2,1)}), bf16[32,24,256]{2,1,0:T(8,128)(2,1)S(1)}, u32[]{:S(2)}, u32[]{:S(2)}) async-start(bf16[32,24,256]{2,1,0:T(8,128)(2,1)} %reduce-scatter.2.cloned.1.call-done), calls=%async_computation.5 | async-start | bytes 786432 | tf_op jit(solution)/shard_map/all_to_all | solution.py:94
  245.4 0.0 copy-done.2
  245.4 0.1 copy.23
  245.6 27.4 %all-to-all-done.4 = bf16[32,24,256]{2,1,0:T(8,128)(2,1)S(1)} async-done(((bf16[32,24,256]{2,1,0:T(8,128)(2,1)}), bf16[32,24,256]{2,1,0:T(8,128)(2,1)S(1)}, u32[]{:S(2)}, u32[]{:S(2)}) %all-to-all-start.4) | async-done | bytes 393248 | tf_op jit(solution)/shard_map/all_to_all | solution.py:94
  272.9 1.9 gather_fusion.1
  274.9 0.3 reshape.108
  275.2 1.4 multiply_reduce_fusion
  (13 shorter events, 0.2 us)
Async XLA Ops:
  6.5 161.8 %copy-start = (bf16[1,384,2048]{2,1,0:T(8,128)(2,1)S(1)}, bf16[1,384,2048]{2,1,0:T(8,128)(2,1)}, u32[]{:S(2)}) copy-start(bf16[1,384,2048]{2,1,0:T(8,128)(2,1)} %param.13) | copy-start | bytes 4718596
  8.3 15.0 %all-to-all-start = ((f32[8,256,1]{1,2,0:T(1,128)}), f32[8,256,1]{1,2,0:T(1,128)S(1)}, u32[]{:S(2)}, u32[]{:S(2)}) async-start(f32[8,256,1]{1,2,0:T(1,128)} %broadcast_in_dim.29), calls=%async_computation | async-start | bytes 16384 | tf_op jit(solution)/shard_map/all_to_all | solution.py:14
  16.2 212.5 %reduce-scatter.2.cloned.1.call-start = ((), (), s32[]{:S(2)}) async-start(), calls=%async_computation.6 | async-start | bytes 3538944 | tf_op jit(solution)/shard_map/reduce_scatter | solution.py:91
  93.3 71.4 %copy-start.1 = (bf16[1,2048,384]{2,1,0:T(8,128)(2,1)S(1)}, bf16[1,2048,384]{2,1,0:T(8,128)(2,1)}, u32[]{:S(2)}) copy-start(bf16[1,2048,384]{2,1,0:T(8,128)(2,1)} %param.11) | copy-start | bytes 4718596
  164.6 1.8 copy-start.3
  171.8 73.6 %copy-start.2 = (f32[256,2]{0,1:T(2,128)S(1)}, f32[256,2]{0,1:T(2,128)}, u32[]{:S(2)}) copy-start(f32[256,2]{0,1:T(2,128)} %param.10) | copy-start | bytes 6148
  228.6 44.3 %all-to-all-start.4 = ((bf16[32,24,256]{2,1,0:T(8,128)(2,1)}), bf16[32,24,256]{2,1,0:T(8,128)(2,1)S(1)}, u32[]{:S(2)}, u32[]{:S(2)}) async-start(bf16[32,24,256]{2,1,0:T(8,128)(2,1)} %reduce-scatter.2.cloned.1.call-done), calls=%async_computation.5 | async-start | bytes 786432 | tf_op jit(solution)/shard_map/all_to_all | solution.py:94
Sparse Core Ops, SparseCore 0:
  172.0 56.5 reduce-scatter.1
